TPU v7x, 512 devices: a whole 4x4x16 slice. The times are simulated.
512 devices in a mesh: fs: 32 (over z, core), tp: 16 (over y, x).
Axes of the slice: x: 4, y: 4, z: 16, core: 2. Of those that a mesh axis runs over, the one named last changes fastest.
Arguments:
- late_input: bfloat16 [4096, 2048], P('fs'), may hold values from -6 to 6
- early_input: bfloat16 [4096, 2048], P('fs'), may hold values from -6 to 6
- early_mid: bfloat16 [4096, 2048], P('fs'), may hold values from -6 to 6
- cotangent: bfloat16 [4096, 2048], P('fs'), may hold values from -6 to 6
- gain_first: float32 [2048], replicated, may hold values from 0.1 to 1.9
- gain_second: float32 [2048], replicated, may hold values from 0.1 to 1.9
- gate_first: bfloat16 [2048, 2816], P('fs', 'tp'), may hold values from -0.125 to 0.125
- up_first: bfloat16 [2048, 2816], P('fs', 'tp'), may hold values from -0.125 to 0.125
- down_first: bfloat16 [2816, 2048], P('tp', 'fs'), may hold values from -0.109375 to 0.109375
- gate_second: bfloat16 [2048, 2816], P('fs', 'tp'), may hold values from -0.125 to 0.125
- up_second: bfloat16 [2048, 2816], P('fs', 'tp'), may hold values from -0.125 to 0.125
- down_second: bfloat16 [2816, 2048], P('tp', 'fs'), may hold values from -0.109375 to 0.109375
- sum_gate_first: float32 [2048, 2816], P('fs', 'tp'), may hold values from -256 to 256
- sum_up_first: float32 [2048, 2816], P('fs', 'tp'), may hold values from -256 to 256
- sum_down_first: float32 [2816, 2048], P('tp', 'fs'), may hold values from -256 to 256
- sum_gate_second: float32 [2048, 2816], P('fs', 'tp'), may hold values from -256 to 256
- sum_up_second: float32 [2048, 2816], P('fs', 'tp'), may hold values from -256 to 256
- sum_down_second: float32 [2816, 2048], P('tp', 'fs'), may hold values from -256 to 256
Outputs:
- late_mid: bfloat16 [4096, 2048], P('fs')
- late_out: bfloat16 [4096, 2048], P('fs')
- input_grad: bfloat16 [4096, 2048], P('fs')
- new_gate_first: float32 [2048, 2816], P('fs', 'tp')
- new_up_first: float32 [2048, 2816], P('fs', 'tp')
- new_down_first: float32 [2816, 2048], P('tp', 'fs')
- new_gate_second: float32 [2048, 2816], P('fs', 'tp')
- new_up_second: float32 [2048, 2816], P('fs', 'tp')
- new_down_second: float32 [2816, 2048], P('tp', 'fs')
All inputs are finite; a program needn't handle non-finite values.
Results may differ from a plain program's by a relative error of at most 0.015.
Values may be sent and summed in bfloat16 or wider, within the bound.
No kernel may reach another device: no remote copies, remote signals or barrier semaphores. Data moves between devices by JAX's collectives and lax.ppermute only.
A program may use at most 128 MiB of HBM per device.

v0:
```python
import jax
import jax.numpy as jnp
from jax import lax
from jax.sharding import PartitionSpec as P

norm_eps = 1e-06


def sent_together(arrays, axis, dim, along):
    both = jnp.concatenate(arrays, axis=along)
    whole, at, outs = (lax.all_gather(both, axis, axis=dim, tiled=True), 0, [])
    for a in arrays:
        outs.append(lax.slice_in_dim(whole, at, at + a.shape[along], axis=along))
        at += a.shape[along]
    return tuple(outs)


def gather_turned(arrays, axis, dims):
    turned = [jnp.moveaxis(a, dim, 0) for a, dim in zip(arrays, dims)]
    widths = [t[0].size for t in turned]
    both = jnp.concatenate([t.reshape(-1, w) for t, w in zip(turned, widths)], axis=1)
    whole = lax.all_gather(both, axis, axis=0, tiled=True)
    blocks = jnp.split(whole, [sum(widths[:k]) for k in range(1, len(widths))], axis=1)
    return tuple(
        (
            jnp.moveaxis(b.reshape(-1, *t.shape[1:]), 0, dim)
            for b, t, dim in zip(blocks, turned, dims)
        )
    )


def normalize(values, gain_vector):
    widened = values.astype(jnp.float32)
    factor = lax.rsqrt(jnp.mean(widened * widened, axis=-1, keepdims=True) + norm_eps)
    normed = (widened * factor * gain_vector).astype(jnp.bfloat16)
    return (widened, factor, normed)


def block_forward(values, params):
    gain_vector, w_gate, w_up, w_down = params
    widened, factor, normed = normalize(values, gain_vector)
    gate_pre = jnp.dot(normed, w_gate, preferred_element_type=jnp.float32)
    up_pre = jnp.dot(normed, w_up, preferred_element_type=jnp.float32)
    hidden = (jax.nn.silu(gate_pre) * up_pre).astype(jnp.bfloat16)
    branch = lax.psum(
        jnp.dot(hidden, w_down, preferred_element_type=jnp.float32).astype(jnp.bfloat16), "tp"
    ).astype(jnp.float32)
    return (widened + 0.5 * branch).astype(jnp.bfloat16)


def block_backward(values, cotangent, params):
    gain_vector, w_gate, w_up, w_down = params
    widened, factor, normed = normalize(values, gain_vector)
    gate_pre = jnp.dot(normed, w_gate, preferred_element_type=jnp.float32)
    up_pre = jnp.dot(normed, w_up, preferred_element_type=jnp.float32)
    sigmoid_gate = jax.nn.sigmoid(gate_pre)
    activated = gate_pre * sigmoid_gate
    hidden = (activated * up_pre).astype(jnp.bfloat16)
    hidden_grad = 0.5 * jnp.einsum(
        "td,fd->tf", cotangent, w_down, preferred_element_type=jnp.float32
    )
    gate_grad = (
        hidden_grad * up_pre * sigmoid_gate * (1.0 + gate_pre * (1.0 - sigmoid_gate))
    ).astype(jnp.bfloat16)
    up_grad = (hidden_grad * activated).astype(jnp.bfloat16)
    partial_value = jnp.einsum("tf,df->td", gate_grad, w_gate, preferred_element_type=jnp.float32)
    partial_value = partial_value + jnp.einsum(
        "tf,df->td", up_grad, w_up, preferred_element_type=jnp.float32
    )
    normed_grad = lax.psum(partial_value.astype(jnp.bfloat16), "tp").astype(jnp.float32)
    scaled = normed_grad * gain_vector
    unit_rows = widened * factor
    rows_grad = cotangent.astype(jnp.float32) + factor * (
        scaled - unit_rows * jnp.mean(scaled * unit_rows, axis=-1, keepdims=True)
    )
    return (rows_grad, (normed, cotangent, gate_grad, up_grad, hidden))


def fold_pair(pieces, columns_in):
    return (
        jnp.einsum("td,tf->df", columns_in, pieces[0], preferred_element_type=jnp.float32),
        jnp.einsum("td,tf->df", columns_in, pieces[1], preferred_element_type=jnp.float32),
    )


def fold_block(pieces, columns_in, columns_out):
    paired = fold_pair(pieces[0:2], columns_in)
    return paired + (
        jnp.einsum("tf,td->fd", pieces[2], columns_out, preferred_element_type=jnp.float32),
    )


def per_device(
    late_input,
    early_input,
    early_mid,
    cotangent,
    gain_first,
    gain_second,
    gate_first,
    up_first,
    down_first,
    gate_second,
    up_second,
    down_second,
    sum_gate_first,
    sum_up_first,
    sum_down_first,
    sum_gate_second,
    sum_up_second,
    sum_down_second,
):
    rows_in = sent_together((gate_first, up_first, gate_second, up_second), "fs", 0, 1)
    cols_out = gather_turned((down_first, down_second), "fs", (1, 1))
    first_params = (gain_first, rows_in[0], rows_in[1], cols_out[0])
    second_params = (gain_second, rows_in[2], rows_in[3], cols_out[1])
    late_mid = block_forward(late_input, first_params)
    late_out = block_forward(late_mid, second_params)
    mid_grad, saved_second = block_backward(early_mid, cotangent, second_params)
    mid_grad = mid_grad.astype(jnp.bfloat16)
    rows_grad, saved_first = block_backward(early_input, mid_grad, first_params)
    pieces = sent_together(
        (
            saved_second[2],
            saved_second[3],
            saved_second[4],
            saved_first[2],
            saved_first[3],
            saved_first[4],
        ),
        "fs",
        0,
        1,
    )
    upper = fold_block(
        pieces[0:3],
        lax.all_to_all(saved_second[0], "fs", split_axis=1, concat_axis=0, tiled=True),
        lax.all_to_all(saved_second[1], "fs", split_axis=1, concat_axis=0, tiled=True),
    )
    lower = fold_block(
        pieces[3:6],
        lax.all_to_all(saved_first[0], "fs", split_axis=1, concat_axis=0, tiled=True),
        lax.all_to_all(saved_first[1], "fs", split_axis=1, concat_axis=0, tiled=True),
    )
    result = upper + lower
    grads_second = (result[0], result[1], 0.5 * result[2])
    grads_first = (result[3], result[4], 0.5 * result[5])
    return (
        late_mid,
        late_out,
        rows_grad.astype(jnp.bfloat16),
        sum_gate_first + grads_first[0],
        sum_up_first + grads_first[1],
        sum_down_first + grads_first[2],
        sum_gate_second + grads_second[0],
        sum_up_second + grads_second[1],
        sum_down_second + grads_second[2],
    )


def solution(mesh):
    in_specs = (
        P("fs", None),
        P("fs", None),
        P("fs", None),
        P("fs", None),
        P(),
        P(),
        P("fs", "tp"),
        P("fs", "tp"),
        P("tp", "fs"),
        P("fs", "tp"),
        P("fs", "tp"),
        P("tp", "fs"),
        P("fs", "tp"),
        P("fs", "tp"),
        P("tp", "fs"),
        P("fs", "tp"),
        P("fs", "tp"),
        P("tp", "fs"),
    )
    out_specs = (
        P("fs", None),
        P("fs", None),
        P("fs", None),
        P("fs", "tp"),
        P("fs", "tp"),
        P("tp", "fs"),
        P("fs", "tp"),
        P("fs", "tp"),
        P("tp", "fs"),
    )
    return jax.shard_map(
        per_device, mesh=mesh, in_specs=in_specs, out_specs=out_specs, check_vma=False
    )
```

profile of v0, /device:TPU:1, one launch (start us, length us, event | category | flops | bytes accessed | tf_op | source)
XLA Modules:
  0.0 560.9 jit_solution(5887314163387625684)
XLA Ops:
  7.2 1.5 pad_maximum_fusion.1
  8.8 1.6 pad_maximum_fusion
  10.4 1.2 fusion.61
  11.6 1.2 fusion.53
  12.9 1.2 fusion.60
  14.1 2.0 fusion.47
  16.1 71.3 %all-gather.6.cloned.1.call-done = bf16[2048,352]{1,0:T(8,128)(2,1)} async-done(((bf16[64,352]{1,0:T(8,128)(2,1)}), bf16[2048,352]{1,0:T(8,128)(2,1)}) %all-gather.6.cloned.1.call-update) | async-done | bytes 1441808 | tf_op jit(solution)/shard_map/all_gather | solution.py:22
  87.5 2.1 fusion.20
  89.6 70.4 %all-gather.4.cloned.1.call-done = bf16[2048,704]{1,0:T(8,128)(2,1)} async-done(((bf16[64,704]{1,0:T(8,128)(2,1)}), bf16[2048,704]{1,0:T(8,128)(2,1)}) %all-gather.4.cloned.1.call-update) | async-done | bytes 2883600 | tf_op jit(solution)/shard_map/all_gather | solution.py:11
  160.0 2.6 fusion.74
  162.6 3.2 constant_dynamic-update-slice_fusion.3
  166.5 1.6 fusion.93
  168.1 3.9 convolution_convert_fusion.1
  172.0 0.7 fusion.78
  172.6 1.5 fusion
  174.4 1.2 fusion.54
  175.6 0.8 fusion.125
  176.5 1.0 fusion.85
  177.5 110.1 %all-reduce.7.cloned.1.call-done = (bf16[128,2048]{1,0:T(8,128)(2,1)}, bf16[128,2048]{1,0:T(8,128)(2,1)}) async-done(((bf16[128,2048]{1,0:T(8,128)(2,1)}, bf16[128,2048]{1,0:T(8,128)(2,1)}), (bf16[128,2048]{1,0:T(8,128)(2,1)}, bf16[128,2048]{1,0:T(8,128)(2,1)})) %all-reduce.7.cloned.1.call-update) | async-done | bytes 1048592 | tf_op jit(solution)/shard_map/psum | solution.py:45
  287.6 1.7 fusion.65
  289.3 1.7 fusion.48
  291.0 1.8 fusion.52
  292.8 0.8 copy-done.2
  294.1 1.1 constant_dynamic-update-slice_fusion.1
  295.9 1.7 fusion.82
  297.6 4.0 convolution_convert_fusion
  302.1 1.5 fusion.1
  304.3 2.1 copy.27
  306.4 14.7 %all-to-all-start = ((bf16[128,32,64]{0,2,1:T(8,128)(2,1)}), bf16[128,32,64]{0,2,1:T(8,128)(2,1)S(1)}, u32[]{:S(2)}, u32[]{:S(2)}) async-start(bf16[128,32,64]{0,2,1:T(8,128)(2,1)} %bitcast.3), calls=%async_computation | async-start | bytes 1048576 | tf_op jit(solution)/shard_map/all_to_all | solution.py:142
  321.1 1.0 copy.31
  322.2 32.5 %all-to-all-done = bf16[128,32,64]{0,2,1:T(8,128)(2,1)S(1)} async-done(((bf16[128,32,64]{0,2,1:T(8,128)(2,1)}), bf16[128,32,64]{0,2,1:T(8,128)(2,1)S(1)}, u32[]{:S(2)}, u32[]{:S(2)}) %all-to-all-start) | async-done | bytes 524320 | tf_op jit(solution)/shard_map/all_to_all | solution.py:142
  354.6 4.2 all-to-all-start.2
  358.8 1.0 copy.29
  359.8 32.5 %all-to-all-done.2 = bf16[128,32,64]{0,2,1:T(8,128)(2,1)S(1)} async-done(((bf16[128,32,64]{0,2,1:T(8,128)(2,1)}), bf16[128,32,64]{0,2,1:T(8,128)(2,1)S(1)}, u32[]{:S(2)}, u32[]{:S(2)}) %all-to-all-start.2) | async-done | bytes 524320 | tf_op jit(solution)/shard_map/all_to_all | solution.py:137
  392.3 5.0 all-to-all-start.1
  397.4 1.0 copy.33
  398.4 22.9 %all-reduce.5.cloned.1.call-done = (bf16[128,2048]{1,0:T(8,128)(2,1)}, bf16[128,2048]{1,0:T(8,128)(2,1)}) async-done(((bf16[128,2048]{1,0:T(8,128)(2,1)}, bf16[128,2048]{1,0:T(8,128)(2,1)}), (bf16[128,2048]{1,0:T(8,128)(2,1)}, bf16[128,2048]{1,0:T(8,128)(2,1)})) %all-reduce.5.cloned.1.call-update) | async-done | bytes 1048592 | tf_op jit(solution)/shard_map/psum | solution.py:45
  421.2 1.4 fusion.55
  422.6 8.3 %all-to-all-done.1 = bf16[128,32,64]{0,2,1:T(8,128)(2,1)} async-done(((bf16[128,32,64]{0,2,1:T(8,128)(2,1)}), bf16[128,32,64]{0,2,1:T(8,128)(2,1)}, u32[]{:S(2)}, u32[]{:S(2)}) %all-to-all-start.1) | async-done | bytes 524320 | tf_op jit(solution)/shard_map/all_to_all | solution.py:143
  430.9 6.1 %all-to-all-start.3 = ((bf16[128,32,64]{0,2,1:T(8,128)(2,1)}), bf16[128,32,64]{0,2,1:T(8,128)(2,1)S(1)}, u32[]{:S(2)}, u32[]{:S(2)}) async-start(bf16[128,32,64]{0,2,1:T(8,128)(2,1)} %bitcast.9), calls=%async_computation.3 | async-start | bytes 1048576 | tf_op jit(solution)/shard_map/all_to_all | solution.py:138
  437.1 2.7 fusion.59
  439.8 98.8 %all-gather.8.cloned.1.call-done = bf16[4096,1056]{0,1:T(8,128)(2,1)} async-done(((bf16[128,1056]{0,1:T(8,128)(2,1)}), bf16[4096,1056]{0,1:T(8,128)(2,1)}) %all-gather.8.cloned.1.call-update) | async-done | bytes 8650768 | tf_op jit(solution)/shard_map/all_gather | solution.py:11
  538.7 2.6 fusion.23
  541.2 2.6 fusion.26
  543.9 2.6 fusion.35
  546.4 2.6 fusion.38
  549.1 2.7 fusion.32
  551.8 2.6 fusion.44
  (59 shorter events, 3.6 us)
Async XLA Ops:
  7.2 80.3 %all-gather.6.cloned.1.call-start = ((), (), s32[]{:S(2)}) async-start(), calls=%async_computation.5 | async-start | bytes 1622016 | tf_op jit(solution)/shard_map/all_gather | solution.py:22
  8.7 151.3 %all-gather.4.cloned.1.call-start = ((), (), s32[]{:S(2)}) async-start(), calls=%async_computation.4 | async-start | bytes 3244032 | tf_op jit(solution)/shard_map/all_gather | solution.py:11
  10.4 277.2 %all-reduce.7.cloned.1.call-start = ((), (), s32[]{:S(2)}) async-start(), calls=%async_computation.8 | async-start | bytes 2097152 | tf_op jit(solution)/shard_map/psum | solution.py:45
  16.1 150.4 %copy-start.12 = (f32[2048]{0:T(1024)S(1)}, f32[2048]{0:T(1024)}, u32[]{:S(2)}) copy-start(f32[2048]{0:T(1024)} %param.22) | copy-start | bytes 24580
  160.0 6.5 %copy-start = (bf16[2048,704]{1,0:T(8,128)(2,1)S(1)}, bf16[2048,704]{1,0:T(8,128)(2,1)}, u32[]{:S(2)}) copy-start(bf16[2048,704]{1,0:T(8,128)(2,1)} %all-gather.4.cloned.1.call-done) | copy-start | bytes 8650756
  174.1 115.2 %copy-start.11 = (f32[2048]{0:T(1024)S(1)}, f32[2048]{0:T(1024)}, u32[]{:S(2)}) copy-start(f32[2048]{0:T(1024)} %param.23) | copy-start | bytes 24580
  174.1 247.1 %all-reduce.5.cloned.1.call-start = ((), (), s32[]{:S(2)}) async-start(), calls=%async_computation.7 | async-start | bytes 2097152 | tf_op jit(solution)/shard_map/psum | solution.py:45
  175.6 0.9 copy-start.5
  287.6 6.0 %copy-start.10 = (bf16[2048,352]{1,0:T(8,128)(2,1)S(1)}, bf16[2048,352]{1,0:T(8,128)(2,1)}, u32[]{:S(2)}) copy-start(bf16[2048,352]{1,0:T(8,128)(2,1)} %all-gather.6.cloned.1.call-done) | copy-start | bytes 4325380
  287.6 6.5 %copy-start.6 = (bf16[128,2048]{1,0:T(8,128)(2,1)S(1)}, bf16[128,2048]{1,0:T(8,128)(2,1)}, u32[]{:S(2)}) copy-start(bf16[128,2048]{1,0:T(8,128)(2,1)} %copy-done.5) | copy-start | bytes 1572868
  289.2 6.6 %copy-start.8 = (bf16[128,2048]{1,0:T(8,128)(2,1)}, bf16[128,2048]{1,0:T(8,128)(2,1)S(1)}, u32[]{:S(2)}) copy-start(bf16[128,2048]{1,0:T(8,128)(2,1)S(1)} %get-tuple-element.22) | copy-start | bytes 1572868
  292.8 0.8 copy-start.2
  303.5 17.6 %copy-start.4 = (bf16[128,2048]{1,0:T(8,128)(2,1)S(1)}, bf16[128,2048]{1,0:T(8,128)(2,1)}, u32[]{:S(2)}) copy-start(bf16[128,2048]{1,0:T(8,128)(2,1)} %fusion.47) | copy-start | bytes 1572868
  303.5 55.3 %copy-start.3 = (bf16[128,2048]{1,0:T(8,128)(2,1)S(1)}, bf16[128,2048]{1,0:T(8,128)(2,1)}, u32[]{:S(2)}) copy-start(bf16[128,2048]{1,0:T(8,128)(2,1)} %copy-done.2) | copy-start | bytes 1572868
  303.6 235.1 %all-gather.8.cloned.1.call-start = ((), (), s32[]{:S(2)}) async-start(), calls=%async_computation.6 | async-start | bytes 8921088 | tf_op jit(solution)/shard_map/all_gather | solution.py:11
  304.3 93.1 %copy-start.7 = (bf16[128,2048]{1,0:T(8,128)(2,1)S(1)}, bf16[128,2048]{1,0:T(8,128)(2,1)}, u32[]{:S(2)}) copy-start(bf16[128,2048]{1,0:T(8,128)(2,1)} %param.21) | copy-start | bytes 1572868
  306.4 114.8 %copy-start.1 = (bf16[128,2048]{1,0:T(8,128)(2,1)S(1)}, bf16[128,2048]{1,0:T(8,128)(2,1)}, u32[]{:S(2)}) copy-start(bf16[128,2048]{1,0:T(8,128)(2,1)} %param.19) | copy-start | bytes 1572868
  306.4 48.2 %all-to-all-start = ((bf16[128,32,64]{0,2,1:T(8,128)(2,1)}), bf16[128,32,64]{0,2,1:T(8,128)(2,1)S(1)}, u32[]{:S(2)}, u32[]{:S(2)}) async-start(bf16[128,32,64]{0,2,1:T(8,128)(2,1)} %bitcast.3), calls=%async_computation | async-start | bytes 1048576 | tf_op jit(solution)/shard_map/all_to_all | solution.py:142
  354.6 82.4 %copy-start.9 = (bf16[128,2048]{1,0:T(8,128)(2,1)S(1)}, bf16[128,2048]{1,0:T(8,128)(2,1)}, u32[]{:S(2)}) copy-start(bf16[128,2048]{1,0:T(8,128)(2,1)} %copy-done.8) | copy-start | bytes 1572868
  354.6 37.7 %all-to-all-start.2 = ((bf16[128,32,64]{0,2,1:T(8,128)(2,1)}), bf16[128,32,64]{0,2,1:T(8,128)(2,1)S(1)}, u32[]{:S(2)}, u32[]{:S(2)}) async-start(bf16[128,32,64]{0,2,1:T(8,128)(2,1)} %bitcast.7), calls=%async_computation.2 | async-start | bytes 1048576 | tf_op jit(solution)/shard_map/all_to_all | solution.py:137
  392.3 38.6 %all-to-all-start.1 = ((bf16[128,32,64]{0,2,1:T(8,128)(2,1)}), bf16[128,32,64]{0,2,1:T(8,128)(2,1)}, u32[]{:S(2)}, u32[]{:S(2)}) async-start(bf16[128,32,64]{0,2,1:T(8,128)(2,1)} %bitcast.5), calls=%async_computation.1 | async-start | bytes 1048576 | tf_op jit(solution)/shard_map/all_to_all | solution.py:143
  398.4 140.3 %copy-start.13 = (f32[64,176]{1,0:T(8,128)S(1)}, f32[64,176]{1,0:T(8,128)}, u32[]{:S(2)}) copy-start(f32[64,176]{1,0:T(8,128)} %param.30) | copy-start | bytes 135172
  430.9 120.8 %all-to-all-start.3 = ((bf16[128,32,64]{0,2,1:T(8,128)(2,1)}), bf16[128,32,64]{0,2,1:T(8,128)(2,1)S(1)}, u32[]{:S(2)}, u32[]{:S(2)}) async-start(bf16[128,32,64]{0,2,1:T(8,128)(2,1)} %bitcast.9), calls=%async_computation.3 | async-start | bytes 1048576 | tf_op jit(solution)/shard_map/all_to_all | solution.py:138
  437.0 104.2 %copy-start.14 = (f32[64,176]{1,0:T(8,128)S(1)}, f32[64,176]{1,0:T(8,128)}, u32[]{:S(2)}) copy-start(f32[64,176]{1,0:T(8,128)} %param.31) | copy-start | bytes 135172
  439.8 104.0 %copy-start.15 = (f32[64,176]{1,0:T(8,128)S(1)}, f32[64,176]{1,0:T(8,128)}, u32[]{:S(2)}) copy-start(f32[64,176]{1,0:T(8,128)} %param.33) | copy-start | bytes 135172
  439.8 106.6 %copy-start.16 = (f32[64,176]{1,0:T(8,128)S(1)}, f32[64,176]{1,0:T(8,128)}, u32[]{:S(2)}) copy-start(f32[64,176]{1,0:T(8,128)} %param.34) | copy-start | bytes 135172
  541.2 7.8 %copy-start.17 = (f32[176,64]{0,1:T(8,128)S(1)}, f32[176,64]{0,1:T(8,128)}, u32[]{:S(2)}) copy-start(f32[176,64]{0,1:T(8,128)} %param.32) | copy-start | bytes 135172
  546.4 5.3 copy-start.18
Sparse Core Ops, SparseCore 0:
  10.7 76.7 all-gather.5
  90.1 69.8 all-gather.3
  174.2 113.2 all-reduce.6
  303.7 117.5 all-reduce.4
  423.1 115.4 all-gather.7
where the time goes:
time: 562 us; the launch traced here: 561 us
  waiting for transfers between devices  447 us (80%)
  matrix products  41.5 us (7%)
  starting transfers between devices  30.4 us (5%)
  other arithmetic  22 us (4%)
  between operations  14 us (2%)
  local copies, waits for them, and re-layouts  6.1 us (1%)
    all_gather x2, waiting for transfers between devices, sent_together(): whole, at, outs = (lax.all_gather(both, axis, axis=dim, tiled=True), 0, [])  169 us
    psum x2, waiting for transfers between devices, block_forward(): lax.psum(jnp.dot(hidden, w_down, preferred_element_type=jnp.float32).asty...  133 us
    all_gather x1, waiting for transfers between devices, gather_turned(): whole = lax.all_gather(both, axis, axis=0, tiled=True)  71.3 us
    all_to_all x1, waiting for transfers between devices, per_device(): lax.all_to_all(saved_second[0], 'fs', split_axis=1, concat_axis=0, tiled=...  32.5 us
    all_to_all x1, waiting for transfers between devices, per_device(): lax.all_to_all(saved_first[0], 'fs', split_axis=1, concat_axis=0, tiled=T...  32.5 us
    all_to_all x1, starting transfers between devices, per_device(): lax.all_to_all(saved_first[0], 'fs', split_axis=1, concat_axis=0, tiled=T...  14.7 us
  transfers between devices with their start and end apart: 9, of which 8 were waited for; matrix products, arithmetic and copies ran while one was open for 6% of the time, Pallas kernels for 0%

commit v1 on v0

--- a/solution.py
+++ b/solution.py
@@ -19,7 +19,9 @@
     turned = [jnp.moveaxis(a, dim, 0) for a, dim in zip(arrays, dims)]
     widths = [t[0].size for t in turned]
     both = jnp.concatenate([t.reshape(-1, w) for t, w in zip(turned, widths)], axis=1)
-    whole = lax.all_gather(both, axis, axis=0, tiled=True)
+    whole = jnp.concatenate(
+        lax.all_to_all(jnp.stack([both] * lax.axis_size(axis)), axis, 0, 0), axis=0
+    )
     blocks = jnp.split(whole, [sum(widths[:k]) for k in range(1, len(widths))], axis=1)
     return tuple(
         (

time: 562 us -> 531 us (0.945)
  waiting for transfers between devices: 447 us -> 403 us
  starting transfers between devices: 30.4 us -> 47 us
    all_to_all x0 -> x1, waiting for transfers between devices: none -> 82.9 us  [gather_turned(): lax.all_to_all(jnp.stack([both] * lax.axis_size(axis)), axis, 0, 0)]
    all_gather x1 -> x0, waiting for transfers between devices: 71.3 us -> none  [gather_turned(): whole = lax.all_gather(both, axis, axis=0, tiled=True)]
    all_gather x2, waiting for transfers between devices: 169 us -> 113 us  [sent_together(): whole, at, outs = (lax.all_gather(both, axis, axis=dim, tiled=True), 0, [])]
    all_to_all x0 -> x1, starting transfers between devices: none -> 16.7 us  [gather_turned(): lax.all_to_all(jnp.stack([both] * lax.axis_size(axis)), axis, 0, 0)]
where the time goes in v1:
time: 531 us; the launch traced here: 530 us
  waiting for transfers between devices  403 us (76%)
  starting transfers between devices  47 us (9%)
  matrix products  41.5 us (8%)
  other arithmetic  16.5 us (3%)
  between operations  14.1 us (3%)
  local copies, waits for them, and re-layouts  7.52 us (1%)
    psum x2, waiting for transfers between devices, block_forward(): lax.psum(jnp.dot(hidden, w_down, preferred_element_type=jnp.float32).asty...  134 us
    all_gather x2, waiting for transfers between devices, sent_together(): whole, at, outs = (lax.all_gather(both, axis, axis=dim, tiled=True), 0, [])  113 us
    all_to_all x1, waiting for transfers between devices, gather_turned(): lax.all_to_all(jnp.stack([both] * lax.axis_size(axis)), axis, 0, 0)  82.9 us
    all_to_all x1, waiting for transfers between devices, per_device(): lax.all_to_all(saved_second[0], 'fs', split_axis=1, concat_axis=0, tiled=...  32.5 us
    all_to_all x1, waiting for transfers between devices, per_device(): lax.all_to_all(saved_first[0], 'fs', split_axis=1, concat_axis=0, tiled=T...  32.5 us
    all_to_all x1, starting transfers between devices, gather_turned(): lax.all_to_all(jnp.stack([both] * lax.axis_size(axis)), axis, 0, 0)  16.7 us
    all_to_all x1, starting transfers between devices, per_device(): lax.all_to_all(saved_first[0], 'fs', split_axis=1, concat_axis=0, tiled=T...  14.7 us
  transfers between devices with their start and end apart: 9, of which 8 were waited for; matrix products, arithmetic and copies ran while one was open for 6% of the time, Pallas kernels for 0%

profile of v1, /device:TPU:1, one launch (start us, length us, event | category | flops | bytes accessed | tf_op | source)
XLA Modules:
  0.0 529.8 jit_solution(63431844227966916)
XLA Ops:
  7.3 1.0 pad_maximum_fusion.1
  8.2 1.4 stack.2
  9.6 16.7 %all-to-all-start = ((bf16[32,64,352]{2,1,0:T(8,128)(2,1)}), bf16[32,64,352]{2,1,0:T(8,128)(2,1)S(1)}, u32[]{:S(2)}, u32[]{:S(2)}) async-start(bf16[32,64,352]{2,1,0:T(8,128)(2,1)} %stack.2), calls=%async_computation | async-start | bytes 3145728 | tf_op jit(solution)/shard_map/all_to_all | solution.py:23
  26.5 0.7 pad_maximum_fusion
  27.9 1.0 fusion.47
  28.9 82.9 %all-to-all-done = bf16[32,64,352]{2,1,0:T(8,128)(2,1)S(1)} async-done(((bf16[32,64,352]{2,1,0:T(8,128)(2,1)}), bf16[32,64,352]{2,1,0:T(8,128)(2,1)S(1)}, u32[]{:S(2)}, u32[]{:S(2)}) %all-to-all-start) | async-done | bytes 1441824 | tf_op jit(solution)/shard_map/all_to_all | solution.py:23
  111.8 2.2 fusion.20
  114.0 14.1 %all-gather.3.cloned.1.call-done = bf16[2048,704]{1,0:T(8,128)(2,1)} async-done(((bf16[64,704]{1,0:T(8,128)(2,1)}), bf16[2048,704]{1,0:T(8,128)(2,1)}) %all-gather.3.cloned.1.call-update) | async-done | bytes 2883600 | tf_op jit(solution)/shard_map/all_gather | solution.py:11
  128.1 2.6 fusion.74
  130.7 3.2 constant_dynamic-update-slice_fusion.3
  134.6 1.6 fusion.93
  136.2 3.9 convolution_convert_fusion.1
  140.1 0.7 fusion.78
  140.7 1.5 fusion
  142.5 1.2 fusion.54
  143.7 0.7 fusion.125
  144.5 1.0 fusion.85
  145.6 110.9 %all-reduce.7.cloned.1.call-done = (bf16[128,2048]{1,0:T(8,128)(2,1)}, bf16[128,2048]{1,0:T(8,128)(2,1)}) async-done(((bf16[128,2048]{1,0:T(8,128)(2,1)}, bf16[128,2048]{1,0:T(8,128)(2,1)}), (bf16[128,2048]{1,0:T(8,128)(2,1)}, bf16[128,2048]{1,0:T(8,128)(2,1)})) %all-reduce.7.cloned.1.call-update) | async-done | bytes 1048592 | tf_op jit(solution)/shard_map/psum | solution.py:47
  256.5 1.7 fusion.65
  258.2 1.7 fusion.48
  259.9 1.8 fusion.52
  261.7 0.8 copy-done.4
  263.0 1.1 constant_dynamic-update-slice_fusion.1
  264.8 1.7 fusion.82
  266.5 4.0 convolution_convert_fusion
  271.0 1.5 fusion.1
  272.5 0.7 fusion.126
  273.2 2.1 copy.27
  275.3 14.7 %all-to-all-start.1 = ((bf16[128,32,64]{0,2,1:T(8,128)(2,1)}), bf16[128,32,64]{0,2,1:T(8,128)(2,1)S(1)}, u32[]{:S(2)}, u32[]{:S(2)}) async-start(bf16[128,32,64]{0,2,1:T(8,128)(2,1)} %bitcast.4), calls=%async_computation.1 | async-start | bytes 1048576 | tf_op jit(solution)/shard_map/all_to_all | solution.py:144
  290.0 1.0 copy.31
  291.0 32.5 %all-to-all-done.1 = bf16[128,32,64]{0,2,1:T(8,128)(2,1)S(1)} async-done(((bf16[128,32,64]{0,2,1:T(8,128)(2,1)}), bf16[128,32,64]{0,2,1:T(8,128)(2,1)S(1)}, u32[]{:S(2)}, u32[]{:S(2)}) %all-to-all-start.1) | async-done | bytes 524320 | tf_op jit(solution)/shard_map/all_to_all | solution.py:144
  323.5 4.2 all-to-all-start.3
  327.7 1.0 copy.29
  328.7 32.5 %all-to-all-done.3 = bf16[128,32,64]{0,2,1:T(8,128)(2,1)S(1)} async-done(((bf16[128,32,64]{0,2,1:T(8,128)(2,1)}), bf16[128,32,64]{0,2,1:T(8,128)(2,1)S(1)}, u32[]{:S(2)}, u32[]{:S(2)}) %all-to-all-start.3) | async-done | bytes 524320 | tf_op jit(solution)/shard_map/all_to_all | solution.py:139
  361.2 5.0 all-to-all-start.2
  366.3 1.0 copy.33
  367.3 22.9 %all-reduce.5.cloned.1.call-done = (bf16[128,2048]{1,0:T(8,128)(2,1)}, bf16[128,2048]{1,0:T(8,128)(2,1)}) async-done(((bf16[128,2048]{1,0:T(8,128)(2,1)}, bf16[128,2048]{1,0:T(8,128)(2,1)}), (bf16[128,2048]{1,0:T(8,128)(2,1)}, bf16[128,2048]{1,0:T(8,128)(2,1)})) %all-reduce.5.cloned.1.call-update) | async-done | bytes 1048592 | tf_op jit(solution)/shard_map/psum | solution.py:47
  390.1 1.4 fusion.55
  391.5 8.3 %all-to-all-done.2 = bf16[128,32,64]{0,2,1:T(8,128)(2,1)} async-done(((bf16[128,32,64]{0,2,1:T(8,128)(2,1)}), bf16[128,32,64]{0,2,1:T(8,128)(2,1)}, u32[]{:S(2)}, u32[]{:S(2)}) %all-to-all-start.2) | async-done | bytes 524320 | tf_op jit(solution)/shard_map/all_to_all | solution.py:145
  399.8 6.1 %all-to-all-start.4 = ((bf16[128,32,64]{0,2,1:T(8,128)(2,1)}), bf16[128,32,64]{0,2,1:T(8,128)(2,1)S(1)}, u32[]{:S(2)}, u32[]{:S(2)}) async-start(bf16[128,32,64]{0,2,1:T(8,128)(2,1)} %bitcast.10), calls=%async_computation.4 | async-start | bytes 1048576 | tf_op jit(solution)/shard_map/all_to_all | solution.py:140
  406.0 2.7 fusion.59
  408.7 98.8 %all-gather.5.cloned.1.call-done = bf16[4096,1056]{0,1:T(8,128)(2,1)} async-done(((bf16[128,1056]{0,1:T(8,128)(2,1)}), bf16[4096,1056]{0,1:T(8,128)(2,1)}) %all-gather.5.cloned.1.call-update) | async-done | bytes 8650768 | tf_op jit(solution)/shard_map/all_gather | solution.py:11
  507.5 2.6 fusion.23
  510.1 2.6 fusion.26
  512.7 2.6 fusion.35
  515.3 2.6 fusion.38
  518.0 2.7 fusion.32
  520.7 2.6 fusion.44
  (75 shorter events, 3.5 us)
Async XLA Ops:
  7.2 19.2 %copy-start.17 = (bf16[64,176]{1,0:T(8,128)(2,1)S(1)}, bf16[64,176]{1,0:T(8,128)(2,1)}, u32[]{:S(2)}) copy-start(bf16[64,176]{1,0:T(8,128)(2,1)} %param.28) | copy-start | bytes 67588
  7.2 19.2 %copy-start.18 = (bf16[64,176]{1,0:T(8,128)(2,1)S(1)}, bf16[64,176]{1,0:T(8,128)(2,1)}, u32[]{:S(2)}) copy-start(bf16[64,176]{1,0:T(8,128)(2,1)} %param.27) | copy-start | bytes 67588
  7.2 19.2 %copy-start.19 = (bf16[64,176]{1,0:T(8,128)(2,1)S(1)}, bf16[64,176]{1,0:T(8,128)(2,1)}, u32[]{:S(2)}) copy-start(bf16[64,176]{1,0:T(8,128)(2,1)} %param.25) | copy-start | bytes 67588
  7.2 19.2 %copy-start.20 = (bf16[64,176]{1,0:T(8,128)(2,1)S(1)}, bf16[64,176]{1,0:T(8,128)(2,1)}, u32[]{:S(2)}) copy-start(bf16[64,176]{1,0:T(8,128)(2,1)} %param.24) | copy-start | bytes 67588
  7.2 20.1 %copy-start.11 = (bf16[128,2048]{1,0:T(8,128)(2,1)S(1)}, bf16[128,2048]{1,0:T(8,128)(2,1)}, u32[]{:S(2)}) copy-start(bf16[128,2048]{1,0:T(8,128)(2,1)} %param.18) | copy-start | bytes 1572868
  7.2 20.3 %copy-start.1 = (bf16[128,2048]{1,0:T(8,128)(2,1)S(1)}, bf16[128,2048]{1,0:T(8,128)(2,1)}, u32[]{:S(2)}) copy-start(bf16[128,2048]{1,0:T(8,128)(2,1)} %param.20) | copy-start | bytes 1572868
  7.2 20.4 %copy-start.2 = (bf16[128,2048]{1,0:T(8,128)(2,1)S(1)}, bf16[128,2048]{1,0:T(8,128)(2,1)}, u32[]{:S(2)}) copy-start(bf16[128,2048]{1,0:T(8,128)(2,1)} %param.19) | copy-start | bytes 1572868
  8.2 19.7 %copy-start.15 = (f32[2048]{0:T(1024)S(1)}, f32[2048]{0:T(1024)}, u32[]{:S(2)}) copy-start(f32[2048]{0:T(1024)} %param.23) | copy-start | bytes 24580
  9.6 102.2 %all-to-all-start = ((bf16[32,64,352]{2,1,0:T(8,128)(2,1)}), bf16[32,64,352]{2,1,0:T(8,128)(2,1)S(1)}, u32[]{:S(2)}, u32[]{:S(2)}) async-start(bf16[32,64,352]{2,1,0:T(8,128)(2,1)} %stack.2), calls=%async_computation | async-start | bytes 3145728 | tf_op jit(solution)/shard_map/all_to_all | solution.py:23
  26.4 101.8 %all-gather.3.cloned.1.call-start = ((), (), s32[]{:S(2)}) async-start(), calls=%async_computation.5 | async-start | bytes 3244032 | tf_op jit(solution)/shard_map/all_gather | solution.py:11
  27.2 229.2 %all-reduce.7.cloned.1.call-start = ((), (), s32[]{:S(2)}) async-start(), calls=%async_computation.8 | async-start | bytes 2097152 | tf_op jit(solution)/shard_map/psum | solution.py:47
  28.9 105.7 %copy-start.16 = (f32[2048]{0:T(1024)S(1)}, f32[2048]{0:T(1024)}, u32[]{:S(2)}) copy-start(f32[2048]{0:T(1024)} %param.22) | copy-start | bytes 24580
  111.8 2.2 copy-start.9
  128.1 6.5 %copy-start = (bf16[2048,704]{1,0:T(8,128)(2,1)S(1)}, bf16[2048,704]{1,0:T(8,128)(2,1)}, u32[]{:S(2)}) copy-start(bf16[2048,704]{1,0:T(8,128)(2,1)} %all-gather.3.cloned.1.call-done) | copy-start | bytes 8650756
  142.2 247.9 %all-reduce.5.cloned.1.call-start = ((), (), s32[]{:S(2)}) async-start(), calls=%async_computation.7 | async-start | bytes 2097152 | tf_op jit(solution)/shard_map/psum | solution.py:47
  143.7 0.8 copy-start.7
  256.5 6.0 %copy-start.10 = (bf16[32,64,352]{2,1,0:T(8,128)(2,1)S(1)}, bf16[32,64,352]{2,1,0:T(8,128)(2,1)}, u32[]{:S(2)}) copy-start(bf16[32,64,352]{2,1,0:T(8,128)(2,1)} %copy-done.9) | copy-start | bytes 4325380
  256.5 6.5 %copy-start.8 = (bf16[128,2048]{1,0:T(8,128)(2,1)S(1)}, bf16[128,2048]{1,0:T(8,128)(2,1)}, u32[]{:S(2)}) copy-start(bf16[128,2048]{1,0:T(8,128)(2,1)} %copy-done.7) | copy-start | bytes 1572868
  258.1 6.6 %copy-start.13 = (bf16[128,2048]{1,0:T(8,128)(2,1)}, bf16[128,2048]{1,0:T(8,128)(2,1)S(1)}, u32[]{:S(2)}) copy-start(bf16[128,2048]{1,0:T(8,128)(2,1)S(1)} %get-tuple-element.22) | copy-start | bytes 1572868
  261.7 0.8 copy-start.4
  272.4 17.6 %copy-start.6 = (bf16[128,2048]{1,0:T(8,128)(2,1)S(1)}, bf16[128,2048]{1,0:T(8,128)(2,1)}, u32[]{:S(2)}) copy-start(bf16[128,2048]{1,0:T(8,128)(2,1)} %fusion.47) | copy-start | bytes 1572868
  272.4 55.3 %copy-start.5 = (bf16[128,2048]{1,0:T(8,128)(2,1)S(1)}, bf16[128,2048]{1,0:T(8,128)(2,1)}, u32[]{:S(2)}) copy-start(bf16[128,2048]{1,0:T(8,128)(2,1)} %copy-done.4) | copy-start | bytes 1572868
  272.5 235.1 %all-gather.5.cloned.1.call-start = ((), (), s32[]{:S(2)}) async-start(), calls=%async_computation.6 | async-start | bytes 8921088 | tf_op jit(solution)/shard_map/all_gather | solution.py:11
  273.2 93.0 %copy-start.12 = (bf16[128,2048]{1,0:T(8,128)(2,1)S(1)}, bf16[128,2048]{1,0:T(8,128)(2,1)}, u32[]{:S(2)}) copy-start(bf16[128,2048]{1,0:T(8,128)(2,1)} %param.21) | copy-start | bytes 1572868
  275.3 114.8 %copy-start.3 = (bf16[128,2048]{1,0:T(8,128)(2,1)S(1)}, bf16[128,2048]{1,0:T(8,128)(2,1)}, u32[]{:S(2)}) copy-start(bf16[128,2048]{1,0:T(8,128)(2,1)} %param.19) | copy-start | bytes 1572868
  275.3 48.2 %all-to-all-start.1 = ((bf16[128,32,64]{0,2,1:T(8,128)(2,1)}), bf16[128,32,64]{0,2,1:T(8,128)(2,1)S(1)}, u32[]{:S(2)}, u32[]{:S(2)}) async-start(bf16[128,32,64]{0,2,1:T(8,128)(2,1)} %bitcast.4), calls=%async_computation.1 | async-start | bytes 1048576 | tf_op jit(solution)/shard_map/all_to_all | solution.py:144
  323.5 82.4 %copy-start.14 = (bf16[128,2048]{1,0:T(8,128)(2,1)S(1)}, bf16[128,2048]{1,0:T(8,128)(2,1)}, u32[]{:S(2)}) copy-start(bf16[128,2048]{1,0:T(8,128)(2,1)} %copy-done.13) | copy-start | bytes 1572868
  323.5 37.7 %all-to-all-start.3 = ((bf16[128,32,64]{0,2,1:T(8,128)(2,1)}), bf16[128,32,64]{0,2,1:T(8,128)(2,1)S(1)}, u32[]{:S(2)}, u32[]{:S(2)}) async-start(bf16[128,32,64]{0,2,1:T(8,128)(2,1)} %bitcast.8), calls=%async_computation.3 | async-start | bytes 1048576 | tf_op jit(solution)/shard_map/all_to_all | solution.py:139
  361.2 38.6 %all-to-all-start.2 = ((bf16[128,32,64]{0,2,1:T(8,128)(2,1)}), bf16[128,32,64]{0,2,1:T(8,128)(2,1)}, u32[]{:S(2)}, u32[]{:S(2)}) async-start(bf16[128,32,64]{0,2,1:T(8,128)(2,1)} %bitcast.6), calls=%async_computation.2 | async-start | bytes 1048576 | tf_op jit(solution)/shard_map/all_to_all | solution.py:145
  367.3 140.3 %copy-start.21 = (f32[64,176]{1,0:T(8,128)S(1)}, f32[64,176]{1,0:T(8,128)}, u32[]{:S(2)}) copy-start(f32[64,176]{1,0:T(8,128)} %param.30) | copy-start | bytes 135172
  399.8 120.8 %all-to-all-start.4 = ((bf16[128,32,64]{0,2,1:T(8,128)(2,1)}), bf16[128,32,64]{0,2,1:T(8,128)(2,1)S(1)}, u32[]{:S(2)}, u32[]{:S(2)}) async-start(bf16[128,32,64]{0,2,1:T(8,128)(2,1)} %bitcast.10), calls=%async_computation.4 | async-start | bytes 1048576 | tf_op jit(solution)/shard_map/all_to_all | solution.py:140
  405.9 104.2 %copy-start.22 = (f32[64,176]{1,0:T(8,128)S(1)}, f32[64,176]{1,0:T(8,128)}, u32[]{:S(2)}) copy-start(f32[64,176]{1,0:T(8,128)} %param.31) | copy-start | bytes 135172
  408.7 104.0 %copy-start.23 = (f32[64,176]{1,0:T(8,128)S(1)}, f32[64,176]{1,0:T(8,128)}, u32[]{:S(2)}) copy-start(f32[64,176]{1,0:T(8,128)} %param.33) | copy-start | bytes 135172
  408.7 106.6 %copy-start.24 = (f32[64,176]{1,0:T(8,128)S(1)}, f32[64,176]{1,0:T(8,128)}, u32[]{:S(2)}) copy-start(f32[64,176]{1,0:T(8,128)} %param.34) | copy-start | bytes 135172
  510.1 7.8 %copy-start.25 = (f32[176,64]{0,1:T(8,128)S(1)}, f32[176,64]{0,1:T(8,128)}, u32[]{:S(2)}) copy-start(f32[176,64]{0,1:T(8,128)} %param.32) | copy-start | bytes 135172
  515.3 5.3 %copy-start.26 = (f32[176,64]{0,1:T(8,128)S(1)}, f32[176,64]{0,1:T(8,128)}, u32[]{:S(2)}) copy-start(f32[176,64]{0,1:T(8,128)} %param.35) | copy-start | bytes 135172
Sparse Core Ops, SparseCore 0:
  29.9 98.2 all-gather.2
  142.3 114.0 all-reduce.6
  272.6 117.5 all-reduce.4
  392.0 115.4 all-gather.4
